TPU v7x, 32 devices: a whole 2x2x4 slice. The times are simulated.
32 devices in a mesh: ep: 8 (over z, x), tp: 4 (over y, core).
Axes of the slice: x: 2, y: 2, z: 4, core: 2. Of those that a mesh axis runs over, the one named last changes fastest.
Arguments:
- tokens: bfloat16 [192, 3072], P('ep'), may hold values from -6 to 6
- norm_gain: float32 [3072], replicated, may hold values from 0.1 to 1.9
- routing: int32 [192, 4], P('ep'), may hold values from 0 to 7, all different within a row; in each aligned block of 24 rows (0 to 23, 24 to 47, ...) at most 13 rows name the same one
- route_weight: float32 [192, 4], P('ep'), may hold values from 0.05 to 1
- w_gate: bfloat16 [8, 3072, 3072], P('ep', None, 'tp'), may hold values from -0.3125 to 0.3125
- w_up: bfloat16 [8, 3072, 3072], P('ep', None, 'tp'), may hold values from -0.3125 to 0.3125
- w_down: bfloat16 [8, 3072, 3072], P('ep', 'tp'), may hold values from -0.01953125 to 0.01953125
Outputs:
- mixed: bfloat16 [192, 3072], P('ep', 'tp')
Inputs may be any that keep to these rules, and one draw needn't show every extreme that they name: `routing`: each row names 4 different experts. Within the rows of one device (aligned blocks of 24 rows) no expert is named by more than 13 rows, a bound that some block reaches.
All inputs are finite; a program needn't handle non-finite values.
Results may differ from a plain program's by a relative error of at most 0.019.
Values may be sent and summed in bfloat16 or wider, within the bound.
No kernel may reach another device: no remote copies, remote signals or barrier semaphores. Data moves between devices by JAX's collectives and lax.ppermute only.
A program may use at most 64 MiB of HBM per device.

v0:
```python
import jax
import jax.numpy as jnp
from jax import lax
from jax.sharding import PartitionSpec as P

NORM_EPS = 1e-06
CLAMP_LIMIT = 7.0
SIGMOID_SCALE = 1.702


def slot_index(route_rows, expert_total, capacity):
    flat_ids = route_rows.reshape(-1)
    one_hot = (flat_ids[:, None] == jnp.arange(expert_total, dtype=jnp.int32)[None, :]).astype(
        jnp.int32
    )
    before = jnp.cumsum(one_hot, axis=0) - one_hot
    ranked = jnp.sum(before * one_hot, axis=1)
    return flat_ids * capacity + ranked


def local(tokens, norm_gain, routing, route_weight, w_gate, w_up, w_down):
    tok_count = tokens.shape[0]
    width = tokens.shape[1]
    top_count = routing.shape[1]
    expert_total = lax.axis_size("ep") * w_gate.shape[0]
    capacity = max(2, tok_count * top_count // expert_total + 1)
    slice_width = width // lax.axis_size("tp")
    values = tokens.astype(jnp.float32)
    scaled = values * lax.rsqrt(jnp.mean(values * values, axis=-1, keepdims=True) + NORM_EPS)
    normal = (scaled * norm_gain).astype(jnp.bfloat16)
    dest = slot_index(routing, expert_total, capacity)
    slot_ids = jnp.arange(expert_total * capacity, dtype=jnp.int32)
    select = jnp.sum(dest.reshape(1, tok_count, top_count) == slot_ids[:, None, None], axis=2)
    sending = jnp.dot(
        select.astype(jnp.bfloat16), normal, preferred_element_type=jnp.float32
    ).astype(jnp.bfloat16)
    gate_mat = w_gate[0]
    up_mat = w_up[0]
    down_mat = w_down[0]
    own_share = lax.dynamic_slice_in_dim(
        sending, lax.axis_index("tp") * slice_width, slice_width, 1
    )
    arrived = lax.all_to_all(own_share, "ep", split_axis=0, concat_axis=0, tiled=True)
    pieces = lax.all_gather(arrived, "tp", axis=1, tiled=True)
    gate_pre = jnp.dot(pieces, gate_mat, preferred_element_type=jnp.float32)
    up_pre = jnp.dot(pieces, up_mat, preferred_element_type=jnp.float32)
    gated = jnp.minimum(gate_pre, CLAMP_LIMIT)
    upper = jnp.clip(up_pre, -CLAMP_LIMIT, CLAMP_LIMIT)
    hidden = ((upper + 1.0) * gated * jax.nn.sigmoid(SIGMOID_SCALE * gated)).astype(jnp.bfloat16)
    summed = lax.psum_scatter(
        lax.dot_general(
            down_mat, hidden, (((0,), (1,)), ((), ())), preferred_element_type=jnp.float32
        ).astype(jnp.bfloat16),
        "tp",
        scatter_dimension=0,
        tiled=True,
    )
    back = lax.all_to_all(summed, "ep", split_axis=1, concat_axis=1, tiled=True)
    picked = back[:, dest].reshape(slice_width, tok_count, top_count)
    mixed = jnp.sum(picked.astype(jnp.float32) * route_weight[None, :, :], axis=2)
    return mixed.T.astype(jnp.bfloat16)


def solution(mesh):
    placed = (
        P("ep", None),
        P(),
        P("ep", None),
        P("ep", None),
        P("ep", None, "tp"),
        P("ep", None, "tp"),
        P("ep", "tp", None),
    )
    return jax.shard_map(
        local, mesh=mesh, in_specs=placed, out_specs=P("ep", "tp"), check_vma=False
    )
```

profile of v0, /device:TPU:0, one launch (start us, length us, event | category | flops | bytes accessed | tf_op | source)
XLA Modules:
  0.0 87.3 jit_solution(828306079801427838)
XLA Ops:
  6.5 0.0 reduce-scatter.2.cloned.1.call-start
  6.5 0.8 copy.14
  7.3 0.1 eq.28
  7.4 0.1 fusion.48
  7.5 0.1 reduce_window_sum.11
  7.6 0.2 select_reduce_fusion
  7.8 0.1 reduce_sum.41
  7.9 0.1 copy.16
  8.0 0.1 convert_reduce_fusion
  8.1 1.0 %fusion.37 = f32[24]{0:T(128)S(1)} fusion(bf16[24,3072]{1,0:T(8,128)(2,1)} %param.7), kind=kLoop, calls=%fused_computation.23 | loop fusion | flops 221160 | bytes 147552 | tf_op jit(solution)/shard_map/reduce_sum | solution.py:29
  9.2 1.3 %fusion.44 = bf16[104,3072]{1,0:T(8,128)(2,1)S(1)} fusion(bf16[24,3072]{1,0:T(8,128)(2,1)} %param.7, f32[3072]{0:T(1024)} %param.8, f32[24]{0:T(128)S(1)} %add_rsqrt_fusion, s32[104,24]{0,1:T(8,128)S(1)} %convert_reduce_fusion), kind=kOutput, calls=%fused_computation.32 | convolution fusion | flops 15632832 | bytes 808800 | tf_op jit(solution)/shard_map/dot_general | solution.py:34
  10.5 0.1 all_to_all.16
  10.6 15.0 %all_to_all.24 = bf16[8,13,768]{2,1,0:T(8,128)(2,1)S(1)} all-to-all(bf16[8,13,768]{2,1,0:T(8,128)(2,1)S(1)} %all_to_all.16), channel_id=1, replica_groups=mesh['ep'=8,'tp'=4] {'ep'}, dimensions={0} | all-to-all | bytes 319488 | tf_op jit(solution)/shard_map/all_to_all | solution.py:43
  25.6 0.1 all_to_all.18
  25.7 7.8 %all_gather.3 = bf16[104,3072]{1,0:T(8,128)(2,1)S(1)} all-gather(bf16[104,768]{1,0:T(8,128)(2,1)S(1)} %all_to_all.18), channel_id=1, replica_groups=mesh['ep'=8,'tp'=4] {'tp'}, dimensions={1}, use_global_device_ids=true | all-gather | bytes 798720 | tf_op jit(solution)/shard_map/all_gather | solution.py:44
  33.5 3.2 %fusion.12 = f32[104,768]{1,0:T(8,128)S(1)} fusion(bf16[104,3072]{1,0:T(8,128)(2,1)S(1)} %all_gather.3, bf16[1,3072,768]{2,1,0:T(8,128)(2,1)} %param.11), kind=kOutput, calls=%fused_computation.9 | convolution fusion | flops 490813440 | bytes 5677056 | tf_op jit(solution)/shard_map/dot_general | solution.py:45
  36.7 0.0 copy-start
  36.7 6.5 %fusion.9 = bf16[3072,104]{0,1:T(8,128)(2,1)} fusion(bf16[1,768,3072]{2,1,0:T(8,128)(2,1)} %param.13, f32[104,768]{1,0:T(8,128)S(1)} %fusion.12, bf16[104,3072]{1,0:T(8,128)(2,1)S(1)} %all_gather.3, bf16[1,3072,768]{2,1,0:T(8,128)(2,1)} %param.12), kind=kOutput, calls=%fused_computation.8 | convolution fusion | flops 982505472 | bytes 11034624 | tf_op jit(solution)/shard_map/dot_general | solution.py:51
  43.2 0.0 reduce-scatter.2.cloned.1.call-update
  43.2 0.1 mul.76
  43.3 0.0 copy-done
  43.4 0.1 copy.17
  43.4 20.2 %reduce-scatter.2.cloned.1.call-done = bf16[768,104]{0,1:T(8,128)(2,1)} async-done(((bf16[3072,104]{0,1:T(8,128)(2,1)}), bf16[768,104]{0,1:T(8,128)(2,1)}) %reduce-scatter.2.cloned.1.call-update) | async-done | bytes 159760 | tf_op jit(solution)/shard_map/reduce_scatter | solution.py:50
  63.7 1.6 %all_to_all.19 = bf16[768,8,13]{0,2,1:T(8,128)(2,1)} reshape(bf16[768,104]{0,1:T(8,128)(2,1)} %reduce-scatter.2.cloned.1.call-done) | data formatting | bytes 319488 | tf_op jit(solution)/shard_map/all_to_all | solution.py:58
  65.3 5.5 %all-to-all-start.1 = ((bf16[768,8,13]{0,2,1:T(8,128)(2,1)}), bf16[768,8,13]{0,2,1:T(8,128)(2,1)S(1)}, u32[]{:S(2)}, u32[]{:S(2)}) async-start(bf16[768,8,13]{0,2,1:T(8,128)(2,1)} %all_to_all.19), calls=%async_computation.2 | async-start | bytes 393216 | tf_op jit(solution)/shard_map/all_to_all | solution.py:58
  70.8 7.8 %all-to-all-done.1 = bf16[768,8,13]{0,2,1:T(8,128)(2,1)S(1)} async-done(((bf16[768,8,13]{0,2,1:T(8,128)(2,1)}), bf16[768,8,13]{0,2,1:T(8,128)(2,1)S(1)}, u32[]{:S(2)}, u32[]{:S(2)}) %all-to-all-start.1) | async-done | bytes 159776 | tf_op jit(solution)/shard_map/all_to_all | solution.py:58
  78.6 0.1 all_to_all.21
  78.7 0.8 gather_fusion
  79.5 0.1 reshape.54
  79.6 0.9 multiply_reduce_fusion
  (6 shorter events, 0.1 us)
Async XLA Ops:
  6.5 57.1 %reduce-scatter.2.cloned.1.call-start = ((), (), s32[]{:S(2)}) async-start(), calls=%async_computation.3 | async-start | bytes 798720 | tf_op jit(solution)/shard_map/reduce_scatter | solution.py:50
  36.7 6.7 %copy-start = (f32[24,4]{0,1:T(4,128)S(1)}, f32[24,4]{0,1:T(4,128)}, u32[]{:S(2)}) copy-start(f32[24,4]{0,1:T(4,128)} %param.10) | copy-start | bytes 1156
  65.3 13.3 %all-to-all-start.1 = ((bf16[768,8,13]{0,2,1:T(8,128)(2,1)}), bf16[768,8,13]{0,2,1:T(8,128)(2,1)S(1)}, u32[]{:S(2)}, u32[]{:S(2)}) async-start(bf16[768,8,13]{0,2,1:T(8,128)(2,1)} %all_to_all.19), calls=%async_computation.2 | async-start | bytes 393216 | tf_op jit(solution)/shard_map/all_to_all | solution.py:58
Sparse Core Ops, SparseCore 0:
  43.4 20.2 reduce-scatter.1
where the time goes:
time: 87.7 us; the launch traced here: 87.3 us
  waiting for transfers between devices  28 us (32%)
  blocking collectives  22.9 us (26%)
  between operations  13.5 us (15%)
  matrix products  11 us (13%)
  starting transfers between devices  5.5 us (6%)
  local copies, waits for them, and re-layouts  3.96 us (5%)
  other arithmetic  2.44 us (3%)
    reduce_scatter x1, waiting for transfers between devices, local(): lax.psum_scatter(lax.dot_general(down_mat, hidden, (((0,), (1,)), ((), ()...  20.2 us
    all_to_all x1, blocking collectives, local(): lax.all_to_all(own_share, 'ep', split_axis=0, concat_axis=0, tiled=True)  15 us
    all_gather x1, blocking collectives, local(): pieces = lax.all_gather(arrived, 'tp', axis=1, tiled=True)  7.82 us
    all_to_all x1, waiting for transfers between devices, local(): back = lax.all_to_all(summed, 'ep', split_axis=1, concat_axis=1, tiled=True)  7.77 us
    dot_general x1, matrix products, local(): lax.dot_general(down_mat, hidden, (((0,), (1,)), ((), ())), preferred_ele...  6.54 us
    all_to_all x1, starting transfers between devices, local(): back = lax.all_to_all(summed, 'ep', split_axis=1, concat_axis=1, tiled=True)  5.5 us
    dot_general x1, matrix products, local(): gate_pre = jnp.dot(pieces, gate_mat, preferred_element_type=jnp.float32)  3.18 us
  transfers between devices with their start and end apart: 2, of which 2 were waited for; matrix products, arithmetic and copies ran while one was open for 0% of the time, Pallas kernels for 0%

commit v1 on v0

v1 whole, which is shorter than its diff:
```python
import functools

import jax
import jax.numpy as jnp
from jax import lax
from jax.experimental import pallas as pl
from jax.experimental.pallas import tpu as pltpu
from jax.sharding import Mesh, PartitionSpec as P

NORM_EPS = 1e-06
CLAMP_LIMIT = 7.0
SIGMOID_SCALE = 1.702
CORES = 2
TILE_ROWS = 16
LANES = 128

VMEM = pl.BlockSpec(memory_space=pltpu.VMEM)
SMEM = pl.BlockSpec(memory_space=pltpu.SMEM)


def dot(a, b):
    return jnp.dot(a, b, preferred_element_type=jnp.float32)


def slot_select(routes, slots, pad, tok_count):
    top_count = routes.shape[0]
    row = lax.broadcasted_iota(jnp.int32, (slots, tok_count), 0)
    expert = row // pad
    place = row - expert * pad
    named = [routes[k][None, :] == expert for k in range(top_count)]
    chosen = functools.reduce(jnp.logical_or, named)
    earlier = lax.broadcasted_iota(jnp.int32, (tok_count, tok_count), 0) < lax.broadcasted_iota(
        jnp.int32, (tok_count, tok_count), 1
    )
    rank = dot(chosen.astype(jnp.bfloat16), earlier.astype(jnp.bfloat16))
    here = chosen & (rank == place.astype(jnp.float32))
    return named, here


def gather_kernel(core_ref, tok_ref, gain_ref, route_ref, out_ref, *, pad):
    tok_count = tok_ref.shape[0]
    half = out_ref.shape[1]
    values = tok_ref[...].astype(jnp.float32)
    scale = lax.rsqrt(jnp.mean(values * values, axis=-1, keepdims=True) + NORM_EPS)
    lanes = pl.ds(pl.multiple_of(core_ref[0] * half, half), half)
    own = tok_ref[:, lanes].astype(jnp.float32)
    normal = (own * scale * gain_ref[:, lanes]).astype(jnp.bfloat16)
    _, here = slot_select(route_ref[...], out_ref.shape[0], pad, tok_count)
    out_ref[...] = dot(here.astype(jnp.bfloat16), normal).astype(jnp.bfloat16)


def first_kernel(core_ref, x_ref, gate_ref, up_ref, gate_out, up_out):
    half = x_ref.shape[1]
    rows = pl.ds(pl.multiple_of(core_ref[0] * half, half), half)
    gate_out[...] = dot(x_ref[...], gate_ref[0, rows, :])
    up_out[...] = dot(x_ref[...], up_ref[0, rows, :])


def column_block(down_ref, group, core, width):
    if width % LANES == 0:
        start = (group * CORES + core) * width
        return down_ref[0, :, pl.ds(pl.multiple_of(start, width), width)]
    first, second = [
        down_ref[0, :, (group * CORES + i) * width : (group * CORES + i + 1) * width]
        for i in range(CORES)
    ]
    return jnp.where(core == 0, first, second)


def second_kernel(
    core_ref, x_ref, gate_in, up_in, gate_ref, up_ref, down_ref, hidden_ref, away_ref
):
    half = x_ref.shape[1]
    other = (CORES - 1) - core_ref[0]
    rows = pl.ds(pl.multiple_of(other * half, half), half)
    gate_pre = gate_in[...] + dot(x_ref[...], gate_ref[0, rows, :])
    up_pre = up_in[...] + dot(x_ref[...], up_ref[0, rows, :])
    gated = jnp.minimum(gate_pre, CLAMP_LIMIT)
    upper = jnp.clip(up_pre, -CLAMP_LIMIT, CLAMP_LIMIT)
    hidden = ((upper + 1.0) * gated * jax.nn.sigmoid(SIGMOID_SCALE * gated)).astype(jnp.bfloat16)
    hidden_ref[...] = hidden
    groups, _, width = away_ref.shape
    for group in range(groups):
        block = column_block(down_ref, group, other, width)
        away_ref[group] = dot(hidden, block).astype(jnp.bfloat16)


def third_kernel(core_ref, hidden_ref, down_ref, own_ref):
    groups, _, width = own_ref.shape
    for group in range(groups):
        block = column_block(down_ref, group, core_ref[0], width)
        own_ref[group] = dot(hidden_ref[...], block)


def add_kernel(own_ref, away_ref, out_ref, *, blocks, pad):
    groups, _, width = own_ref.shape
    for group in range(groups):
        total = own_ref[group] + away_ref[group].astype(jnp.float32)
        out_ref[:, group] = total.astype(jnp.bfloat16).reshape(blocks, pad, width)


def combine_kernel(back_ref, route_ref, weight_ref, out_ref, *, pad):
    experts, groups, _, width = back_ref.shape
    tok_count = out_ref.shape[0]
    slots = experts * pad
    named, here = slot_select(route_ref[...], slots, pad, tok_count)
    mix = jnp.zeros((slots, tok_count), jnp.float32)
    for k, at in enumerate(named):
        mix = jnp.where(at & here, weight_ref[k][None, :], mix)
    high = mix.astype(jnp.bfloat16)
    low = (mix - high.astype(jnp.float32)).astype(jnp.bfloat16)
    total = jnp.zeros((tok_count, width), jnp.float32)
    for group in range(groups):
        rows = back_ref[:, group].reshape(slots, width)
        for part in (high, low):
            total += lax.dot_general(
                part, rows, (((0,), (0,)), ((), ())), preferred_element_type=jnp.float32
            )
    out_ref[...] = total.astype(jnp.bfloat16)


def call(kernel, out_shape, args, limit, flops, moved):
    specs = [SMEM if a.dtype == jnp.int32 and a.ndim == 1 else VMEM for a in args]
    return pl.pallas_call(
        kernel,
        out_shape=out_shape,
        in_specs=specs,
        out_specs=jax.tree.map(lambda _: VMEM, out_shape),
        compiler_params=pltpu.CompilerParams(vmem_limit_bytes=limit),
        cost_estimate=pl.CostEstimate(flops=flops, bytes_accessed=moved, transcendentals=0),
    )(*args)


def local(tokens, norm_gain, routing, route_weight, w_gate, w_up, w_down):
    tok_count, width = tokens.shape
    top_count = routing.shape[1]
    blocks = lax.axis_size("ep")
    groups = lax.axis_size("y")
    experts = blocks * w_gate.shape[0]
    hidden_width = w_gate.shape[2]
    capacity = max(2, tok_count * top_count // experts + 1)
    pad = -(-capacity // TILE_ROWS) * TILE_ROWS
    rows = blocks * pad
    half = width // CORES
    share = width // (groups * CORES)
    core = lax.axis_index("core").reshape(1)
    swap = [(i, CORES - 1 - i) for i in range(CORES)]
    routes = routing.T
    weights = route_weight.T
    bf16, f32 = jnp.bfloat16, jnp.float32
    mib = 1 << 20

    sending = call(
        functools.partial(gather_kernel, pad=pad),
        jax.ShapeDtypeStruct((experts * pad, half), bf16),
        (core, tokens, norm_gain.reshape(1, width), routes),
        16 * mib,
        20 * 10**9,
        60 * 10**6,
    )
    own = lax.all_to_all(
        sending.reshape(blocks, pad, half), "ep", split_axis=0, concat_axis=0, tiled=True
    ).reshape(rows, half)
    peer = lax.ppermute(own, "core", swap)
    gate = w_gate
    up = w_up
    down = w_down
    pre = jax.ShapeDtypeStruct((rows, hidden_width), f32)
    step = 2 * rows * half * hidden_width
    gate_part, up_part = call(
        first_kernel, (pre, pre), (core, own, gate, up), 16 * mib, 2 * step, 4 * half * hidden_width
    )
    hidden, away = call(
        second_kernel,
        (
            jax.ShapeDtypeStruct((rows, hidden_width), bf16),
            jax.ShapeDtypeStruct((groups, rows, share), bf16),
        ),
        (core, peer, gate_part, up_part, gate, up, down),
        16 * mib,
        3 * step,
        6 * half * hidden_width,
    )
    arrived = lax.ppermute(away, "core", swap)
    kept = call(
        third_kernel,
        jax.ShapeDtypeStruct((groups, rows, share), f32),
        (core, hidden, down),
        16 * mib,
        step,
        2 * half * hidden_width,
    )
    summed = call(
        functools.partial(add_kernel, blocks=blocks, pad=pad),
        jax.ShapeDtypeStruct((blocks, groups, pad, share), bf16),
        (kept, arrived),
        16 * mib,
        rows * half,
        8 * rows * half,
    )
    back = lax.all_to_all(
        summed.reshape(blocks * groups, pad, share),
        ("ep", "y"),
        split_axis=0,
        concat_axis=0,
        tiled=True,
    ).reshape(blocks, groups, pad, share)
    return call(
        functools.partial(combine_kernel, pad=pad),
        jax.ShapeDtypeStruct((tok_count, share), bf16),
        (back, routes, weights),
        16 * mib,
        4 * rows * tok_count * half,
        4 * rows * half,
    )


def solution(mesh):
    blocks, shares = mesh.devices.shape
    split = Mesh(mesh.devices.reshape(blocks, shares // CORES, CORES), ("ep", "y", "core"))
    tp = ("y", "core")
    placed = (
        P("ep", None),
        P(),
        P("ep", None),
        P("ep", None),
        P("ep", None, tp),
        P("ep", None, tp),
        P("ep", tp, None),
    )
    return jax.shard_map(
        local, mesh=split, in_specs=placed, out_specs=P("ep", tp), check_vma=False
    )
```

time: 87.7 us -> 46 us (0.52)
  waiting for transfers between devices: 28 us -> 2.1 us
  blocking collectives: 22.9 us -> 36.4 us
  between operations: 13.5 us -> 0.08 us
  matrix products: 11 us -> 0 us
  starting transfers between devices: 5.5 us -> 0.07 us
  Pallas kernels: 0 us -> 4.09 us
  other arithmetic: 2.44 us -> 0.01 us
  local copies, waits for them, and re-layouts: 3.96 us -> 2.89 us
    all_to_all x1 -> x2, blocking collectives: 15 us -> 36.4 us  [the longest x1 19.4 us: local(): lax.all_to_all(sending.reshape(blocks, pad, half), 'ep', split_axis=0, co...]
    reduce_scatter x1 -> x0, waiting for transfers between devices: 20.2 us -> none  [local(): lax.psum_scatter(lax.dot_general(down_mat, hidden, (((0,), (1,)), ((), ()...]
    dot_general x3 -> x0, matrix products: 11 us -> none  [the longest x1 6.54 us: local(): lax.dot_general(down_mat, hidden, (((0,), (1,)), ((), ())), preferred_ele...]
    all_gather x1 -> x0, blocking collectives: 7.82 us -> none  [local(): pieces = lax.all_gather(arrived, 'tp', axis=1, tiled=True)]
    all_to_all x1 -> x0, waiting for transfers between devices: 7.77 us -> none  [local(): back = lax.all_to_all(summed, 'ep', split_axis=1, concat_axis=1, tiled=True)]
    all_to_all x1 -> x0, starting transfers between devices: 5.5 us -> none  [local(): back = lax.all_to_all(summed, 'ep', split_axis=1, concat_axis=1, tiled=True)]
    pallas_call x0 -> x6, Pallas kernels: none -> 4.09 us  [call(): pl.pallas_call(kernel, out_shape=out_shape, in_specs=specs, out_specs=jax...]
    reduce_sum x4 -> x0, other arithmetic: 2.18 us -> none  [the longest x1 1.05 us: local(): jnp.mean(values * values, axis=-1, keepdims=True) + NORM_EPS]
  transfers between devices with their start and end apart: 2 -> 2, of which waited for: 2 -> 2; matrix products, arithmetic and copies ran while one was open for 0% -> 0% of each run, Pallas kernels for 0% -> 3%
where the time goes in v1:
time: 46 us; the launch traced here: 45.6 us
  blocking collectives  36.4 us (79%)
  Pallas kernels  4.09 us (9%)
  local copies, waits for them, and re-layouts  2.89 us (6%)
  waiting for transfers between devices  2.1 us (5%)
    all_to_all x1, blocking collectives, local(): lax.all_to_all(sending.reshape(blocks, pad, half), 'ep', split_axis=0, co...  19.4 us
    all_to_all x1, blocking collectives, local(): lax.all_to_all(summed.reshape(blocks * groups, pad, share), ('ep', 'y'),...  17 us
    pallas_call x6, Pallas kernels, call(): pl.pallas_call(kernel, out_shape=out_shape, in_specs=specs, out_specs=jax...  4.09 us
    unnamed x18, local copies, waits for them, and re-layouts  2.89 us
    ppermute x1, waiting for transfers between devices, local(): arrived = lax.ppermute(away, 'core', swap)  1.19 us
  transfers between devices with their start and end apart: 2, of which 2 were waited for; matrix products, arithmetic and copies ran while one was open for 0% of the time, Pallas kernels for 3%

profile of v1, /device:TPU:0, one launch (start us, length us, event | category | flops | bytes accessed | tf_op | source)
XLA Modules:
  0.0 45.6 jit_solution(7556542541741653369)
XLA Ops:
  0.0 0.0 copy-start.2
  0.0 0.7 %copy-done.2 = s32[24,4]{0,1:T(4,128)S(1)} copy-done((s32[24,4]{0,1:T(4,128)S(1)}, s32[24,4]{0,1:T(4,128)}, u32[]{:S(2)}) %copy-start.2) | copy-done | bytes 408
  0.7 0.0 copy-start.5
  0.7 0.9 %copy-done.5 = bf16[24,3072]{1,0:T(8,128)(2,1)S(1)} copy-done((bf16[24,3072]{1,0:T(8,128)(2,1)S(1)}, bf16[24,3072]{1,0:T(8,128)(2,1)}, u32[]{:S(2)}) %copy-start.5) | copy-done | bytes 147480
  1.6 0.0 copy-start.6
  1.6 0.7 %copy-done.6 = f32[3072]{0:T(1024)S(1)} copy-done((f32[3072]{0:T(1024)S(1)}, f32[3072]{0:T(1024)}, u32[]{:S(2)}) %copy-start.6) | copy-done | bytes 12312
  2.3 0.0 copy-start
  2.3 0.0 copy-start.1
  2.3 0.4 shard_map.73
  2.7 19.4 %all_to_all.10 = bf16[8,16,1536]{2,1,0:T(8,128)(2,1)S(1)} all-to-all(bf16[8,16,1536]{2,1,0:T(8,128)(2,1)S(1)} %bitcast.14), channel_id=1, replica_groups=mesh['ep'=8,'y'=2,'core'=2] {'ep'}, dimensions={0} | all-to-all | bytes 786432 | tf_op jit(solution)/shard_map/all_to_all | solution.py:161
  22.1 0.0 slice-start
  22.1 0.0 slice-start.1
  22.1 0.0 collective-permute-start
  22.1 0.0 copy-done
  22.1 0.0 copy-done.1
  22.1 0.8 %shard_map.74 = (f32[128,768]{1,0:T(8,128)S(1)}, f32[128,768]{1,0:T(8,128)S(1)}) custom-call(s32[1]{0:T(128)} %bitcast.core_ref, bf16[128,1536]{1,0:T(8,128)(2,1)S(1)} %bitcast.11, bf16[1,3072,768]{2,1,0:T(8,128)(2,1)S(1)} %copy-done, bf16[1,3072,768]{2,1,0:T(8,128)(2,1)S(1)} %copy-done.1), custom_call_target="tpu_custom_call" | custom-call | flops 603979776 | bytes 4718592 | tf_op jit(solution)/shard_map/pallas_call | solution.py:124
  22.9 0.9 %collective-permute-done.x_ref = bf16[128,1536]{1,0:T(8,128)(2,1)S(1)} collective-permute-done((bf16[128,1536]{1,0:T(8,128)(2,1)S(1)}, bf16[128,1536]{1,0:T(8,128)(2,1)S(1)}, u32[]{:S(2)}, u32[]{:S(2)}) %collective-permute-start) | collective-permute-done | bytes 393248 | tf_op jit(solution)/shard_map/ppermute | solution.py:164
  23.8 0.5 %slice-done = s8[4194304]{0:T(1024)(128)(4,1)S(1)} async-done(((s8[4718592]{0:T(1024)(128)(4,1)}), s8[4194304]{0:T(1024)(128)(4,1)S(1)}, s32[]{:S(2)}) %slice-start) | async-done | bytes 4194328
  24.3 0.1 slice-done.1
  24.4 1.3 %shard_map.75 = (bf16[128,768]{1,0:T(8,128)(2,1)S(1)}, bf16[2,128,768]{2,1,0:T(8,128)(2,1)S(1)}) custom-call(s32[1]{0:T(128)} %bitcast.core_ref, bf16[128,1536]{1,0:T(8,128)(2,1)S(1)} %collective-permute-done.x_ref, f32[128,768]{1,0:T(8,128)S(1)} %get-tuple-element.9.gate_in, f32[128,768]{1,0:T(8,128)S(1)} %get-tuple-element.10.up_in, ...), custom_call_target="tpu_custom_call" | custom-call | flops 905969664 | bytes 7077888 | tf_op jit(solution)/shard_map/pallas_call | solution.py:124
  25.7 0.0 copy-start.3
  25.7 0.0 copy-start.4
  25.7 0.1 collective-permute-start.1
  25.8 0.5 %shard_map.76.own_ref = f32[2,128,768]{2,1,0:T(8,128)S(1)} custom-call(s32[1]{0:T(128)} %bitcast.core_ref, bf16[128,768]{1,0:T(8,128)(2,1)S(1)} %get-tuple-element.11.hidden_ref, bf16[1,768,3072]{2,1,0:T(8,128)(2,1)S(1)} %bitcast.9), custom_call_target="tpu_custom_call" | custom-call | flops 301989888 | bytes 2359296 | tf_op jit(solution)/shard_map/pallas_call | solution.py:124
  26.3 1.2 %collective-permute-done.1.away_ref = bf16[2,128,768]{2,1,0:T(8,128)(2,1)S(1)} collective-permute-done((bf16[2,128,768]{2,1,0:T(8,128)(2,1)S(1)}, bf16[2,128,768]{2,1,0:T(8,128)(2,1)S(1)}, u32[]{:S(2)}, u32[]{:S(2)}) %collective-permute-start.1) | collective-permute-done | bytes 393248 | tf_op jit(solution)/shard_map/ppermute | solution.py:184
  27.5 0.1 shard_map.77
  27.6 17.0 %all_to_all.11 = bf16[16,16,768]{2,1,0:T(8,128)(2,1)S(1)} all-to-all(bf16[16,16,768]{2,1,0:T(8,128)(2,1)S(1)} %bitcast.13), channel_id=1, replica_groups=mesh['ep'=8,'y'=2,'core'=2] {'ep','y'}, dimensions={0} | all-to-all | bytes 786432 | tf_op jit(solution)/shard_map/all_to_all | solution.py:201
  44.6 0.0 copy-done.3
  44.6 0.0 copy-done.4
  44.6 1.0 %shard_map.78 = bf16[24,768]{1,0:T(8,128)(2,1)} custom-call(bf16[8,2,16,768]{3,2,1,0:T(8,128)(2,1)S(1)} %bitcast.12, s32[4,24]{1,0:T(4,128)S(1)} %bitcast.16, f32[4,24]{1,0:T(4,128)S(1)} %bitcast.17), custom_call_target="tpu_custom_call" | custom-call | flops 18874368 | bytes 786432 | tf_op jit(solution)/shard_map/pallas_call | solution.py:124
  (1 shorter events, 0.0 us)
Async XLA Ops:
  0.0 0.7 %copy-start.2 = (s32[24,4]{0,1:T(4,128)S(1)}, s32[24,4]{0,1:T(4,128)}, u32[]{:S(2)}) copy-start(s32[24,4]{0,1:T(4,128)} %param.9) | copy-start | bytes 1156
  0.7 0.9 %copy-start.5 = (bf16[24,3072]{1,0:T(8,128)(2,1)S(1)}, bf16[24,3072]{1,0:T(8,128)(2,1)}, u32[]{:S(2)}) copy-start(bf16[24,3072]{1,0:T(8,128)(2,1)} %tok_ref.1) | copy-start | bytes 442372
  1.6 0.7 %copy-start.6 = (f32[3072]{0:T(1024)S(1)}, f32[3072]{0:T(1024)}, u32[]{:S(2)}) copy-start(f32[3072]{0:T(1024)} %param.8) | copy-start | bytes 36868
  2.3 19.8 %copy-start = (bf16[1,3072,768]{2,1,0:T(8,128)(2,1)S(1)}, bf16[1,3072,768]{2,1,0:T(8,128)(2,1)}, u32[]{:S(2)}) copy-start(bf16[1,3072,768]{2,1,0:T(8,128)(2,1)} %gate_ref.3) | copy-start | bytes 14155780
  2.3 19.8 %copy-start.1 = (bf16[1,3072,768]{2,1,0:T(8,128)(2,1)S(1)}, bf16[1,3072,768]{2,1,0:T(8,128)(2,1)}, u32[]{:S(2)}) copy-start(bf16[1,3072,768]{2,1,0:T(8,128)(2,1)} %up_ref.3) | copy-start | bytes 14155780
  22.1 2.2 %slice-start = ((s8[4718592]{0:T(1024)(128)(4,1)}), s8[4194304]{0:T(1024)(128)(4,1)S(1)}, s32[]{:S(2)}) async-start(s8[4718592]{0:T(1024)(128)(4,1)} %bitcast.8), calls=%async_computation.2 | async-start | bytes 8388608
  22.1 2.3 %slice-start.1 = ((s8[4718592]{0:T(1024)(128)(4,1)}), s8[524288]{0:T(1024)(128)(4,1)S(1)}, s32[]{:S(2)}) async-start(s8[4718592]{0:T(1024)(128)(4,1)} %bitcast.8), calls=%async_computation.3 | async-start | bytes 1048576
  22.1 1.7 %collective-permute-start = (bf16[128,1536]{1,0:T(8,128)(2,1)S(1)}, bf16[128,1536]{1,0:T(8,128)(2,1)S(1)}, u32[]{:S(2)}, u32[]{:S(2)}) collective-permute-start(bf16[128,1536]{1,0:T(8,128)(2,1)S(1)} %bitcast.10), channel_id=1, source_target_pairs={{0,1},{1,0},{2,3},{3,2},{4,5},{5,4},{6,7},{7,6},{8,9},{9,8},{10,11... | collective-permute-start | bytes 1179656 | tf_op jit(solution)/shard_map/ppermute | solution.py:164
  25.7 18.9 %copy-start.3 = (s32[24,4]{0,1:T(4,128)S(1)}, s32[24,4]{0,1:T(4,128)}, u32[]{:S(2)}) copy-start(s32[24,4]{0,1:T(4,128)} %param.9) | copy-start | bytes 1156
  25.7 18.9 %copy-start.4 = (f32[24,4]{0,1:T(4,128)S(1)}, f32[24,4]{0,1:T(4,128)}, u32[]{:S(2)}) copy-start(f32[24,4]{0,1:T(4,128)} %param.10) | copy-start | bytes 1156
  25.7 1.8 %collective-permute-start.1 = (bf16[2,128,768]{2,1,0:T(8,128)(2,1)S(1)}, bf16[2,128,768]{2,1,0:T(8,128)(2,1)S(1)}, u32[]{:S(2)}, u32[]{:S(2)}) collective-permute-start(bf16[2,128,768]{2,1,0:T(8,128)(2,1)S(1)} %get-tuple-element.12), channel_id=1, source_target_pairs={{0,1},{1,0},{2,3},{3,2},{4,5},{5,4},{6,7},{7,6},{8,9},{9,8},{10,11... | collective-permute-start | bytes 1179656 | tf_op jit(solution)/shard_map/ppermute | solution.py:184

commit v2 on v1

v2 whole, which is shorter than its diff:
```python
import functools

import jax
import jax.numpy as jnp
from jax import lax
from jax.experimental import pallas as pl
from jax.experimental.pallas import tpu as pltpu
from jax.sharding import Mesh, PartitionSpec as P

NORM_EPS = 1e-06
CLAMP_LIMIT = 7.0
SIGMOID_SCALE = 1.702
CORES = 2
TILE_ROWS = 16
LANES = 128
MIB = 1 << 20

VMEM = pl.BlockSpec(memory_space=pltpu.VMEM)
SMEM = pl.BlockSpec(memory_space=pltpu.SMEM)
HBM = pl.BlockSpec(memory_space=pltpu.HBM)


def round_up(count, unit):
    return -(-count // unit) * unit


class Wire:
    def __init__(self, messages, capacity, width):
        self.messages = messages
        self.capacity = capacity
        self.pad = round_up(capacity, TILE_ROWS)
        self.lanes = LANES if width % LANES == 0 else width
        self.columns = width // self.lanes
        self.stride = round_up(self.columns * capacity, TILE_ROWS)
        self.rows = messages * self.stride

    def window(self, message, column):
        start = message * self.stride + column * self.capacity
        return slice(start, start + self.pad)

    def block(self, column):
        return slice(column * self.lanes, (column + 1) * self.lanes)

    def scratch(self):
        return pltpu.VMEM((self.rows + self.pad, self.lanes), jnp.float32)

    def pack(self, scratch, out_ref, get):
        blank = jnp.zeros((TILE_ROWS, self.lanes), jnp.float32)
        for message in range(self.messages):
            end = (message + 1) * self.stride
            scratch[end - TILE_ROWS : end, :] = blank
            for column in range(self.columns):
                scratch[self.window(message, column), :] = get(message, column)
        out_ref[...] = scratch[: self.rows, :].astype(jnp.bfloat16)

    def unpack(self, wire_ref, scratch, put):
        scratch[: self.rows, :] = wire_ref[...].astype(jnp.float32)
        scratch[self.rows :, :] = jnp.zeros((self.pad, self.lanes), jnp.float32)
        for message in range(self.messages):
            for column in range(self.columns):
                put(message, column, scratch[self.window(message, column), :].astype(jnp.bfloat16))


def dot(a, b):
    return jnp.dot(a, b, preferred_element_type=jnp.float32)


def gather_kernel(
    core_ref, tok_hbm, gain_hbm, route_hbm, out_ref, tok_ref, gain_ref, route_ref, scratch, sems, *, wire
):
    tok_count, width = tok_ref.shape
    half = width // CORES
    copies = [
        pltpu.make_async_copy(source, target, sems.at[i])
        for i, (source, target) in enumerate(
            ((route_hbm, route_ref), (tok_hbm, tok_ref), (gain_hbm, gain_ref))
        )
    ]
    for copy in copies:
        copy.start()
    copies[0].wait()
    slots = wire.messages * wire.pad
    row = lax.broadcasted_iota(jnp.int32, (slots, tok_count), 0)
    expert = row // wire.pad
    place = (row - expert * wire.pad).astype(jnp.float32)
    chosen = functools.reduce(
        jnp.logical_or, [route_ref[k][None, :] == expert for k in range(route_ref.shape[0])]
    )
    earlier = lax.broadcasted_iota(jnp.int32, (tok_count, tok_count), 0) < lax.broadcasted_iota(
        jnp.int32, (tok_count, tok_count), 1
    )
    rank = dot(chosen.astype(jnp.bfloat16), earlier.astype(jnp.bfloat16))
    select = (chosen & (rank == place)).astype(jnp.bfloat16)
    copies[1].wait()
    values = tok_ref[...].astype(jnp.float32)
    scale = lax.rsqrt(jnp.mean(values * values, axis=-1, keepdims=True) + NORM_EPS)
    copies[2].wait()
    lanes = pl.ds(pl.multiple_of(core_ref[0] * half, half), half)
    own = tok_ref[:, lanes].astype(jnp.float32)
    normal = (own * scale * gain_ref[:, lanes]).astype(jnp.bfloat16)
    rows = dot(select, normal)
    wire.pack(
        scratch,
        out_ref,
        lambda message, column: rows[
            message * wire.pad : (message + 1) * wire.pad, wire.block(column)
        ],
    )


def unpack_rows(wire, wire_ref, scratch, x_ref):
    def put(message, column, rows):
        x_ref[message * wire.pad : (message + 1) * wire.pad, wire.block(column)] = rows

    wire.unpack(wire_ref, scratch, put)


def first_kernel(
    core_ref, wire_ref, gate_ref, up_ref, _, gate_out, up_out, scratch, x_ref, *, wire
):
    unpack_rows(wire, wire_ref, scratch, x_ref)
    half = x_ref.shape[1]
    rows = pl.ds(pl.multiple_of(core_ref[0] * half, half), half)
    gate_out[...] = dot(x_ref[...], gate_ref[0, rows, :])
    up_out[...] = dot(x_ref[...], up_ref[0, rows, :])


def column_block(down_ref, group, core, width):
    if width % LANES == 0:
        start = (group * CORES + core) * width
        return down_ref[0, :, pl.ds(pl.multiple_of(start, width), width)]
    first, second = [
        down_ref[0, :, (group * CORES + i) * width : (group * CORES + i + 1) * width]
        for i in range(CORES)
    ]
    return jnp.where(core == 0, first, second)


def second_kernel(
    core_ref,
    wire_ref,
    gate_in,
    up_in,
    gate_ref,
    up_ref,
    down_ref,
    hidden_ref,
    away_ref,
    scratch,
    x_ref,
    *,
    wire,
):
    unpack_rows(wire, wire_ref, scratch, x_ref)
    half = x_ref.shape[1]
    other = (CORES - 1) - core_ref[0]
    rows = pl.ds(pl.multiple_of(other * half, half), half)
    gate_pre = gate_in[...] + dot(x_ref[...], gate_ref[0, rows, :])
    up_pre = up_in[...] + dot(x_ref[...], up_ref[0, rows, :])
    gated = jnp.minimum(gate_pre, CLAMP_LIMIT)
    upper = jnp.clip(up_pre, -CLAMP_LIMIT, CLAMP_LIMIT)
    hidden = ((upper + 1.0) * gated * jax.nn.sigmoid(SIGMOID_SCALE * gated)).astype(jnp.bfloat16)
    hidden_ref[...] = hidden
    groups, _, width = away_ref.shape
    for group in range(groups):
        block = column_block(down_ref, group, other, width)
        away_ref[group] = dot(hidden, block).astype(jnp.bfloat16)


def turned(eye, table):
    return lax.dot_general(
        eye, table, (((1,), (1,)), ((), ())), preferred_element_type=jnp.float32
    )


def third_kernel(
    core_ref, hidden_ref, down_ref, route_ref, weight_ref, own_ref, mix_ref, *, wire, experts
):
    groups, _, width = own_ref.shape
    for group in range(groups):
        block = column_block(down_ref, group, core_ref[0], width)
        own_ref[group] = dot(hidden_ref[...], block)

    bf16, f32 = jnp.bfloat16, jnp.float32
    top_count, tok_count = route_ref.shape
    square = (tok_count, tok_count)
    down_at = lax.broadcasted_iota(jnp.int32, square, 0)
    across = lax.broadcasted_iota(jnp.int32, square, 1)
    eye = (down_at == across).astype(bf16)
    routes = turned(eye, route_ref[...].astype(bf16)).astype(jnp.int32)
    weights = weight_ref[...]
    high = weights.astype(bf16)
    low = (weights - high.astype(f32)).astype(bf16)
    weights = turned(eye, high) + turned(eye, low)
    lane = lax.broadcasted_iota(jnp.int32, (1, wire.rows), 1)
    message = lane // wire.stride
    offset = (lane - message * wire.stride).astype(f32)
    expert = message // groups
    weight = jnp.zeros((tok_count, wire.rows), f32)
    chosen = jnp.zeros((tok_count, wire.rows), f32)
    for k in range(top_count):
        at = routes[:, k : k + 1] == expert
        weight = jnp.where(at, weights[:, k : k + 1], weight)
        chosen = jnp.where(at, 1.0, chosen)
    rank = dot((across < down_at).astype(bf16), chosen.astype(bf16))
    away = offset - rank
    mix = jnp.concatenate(
        [
            jnp.where(away == float(column * wire.capacity), weight, 0.0)
            for column in range(wire.columns)
        ],
        axis=0,
    )
    high = mix.astype(bf16)
    mix_ref[0] = high
    mix_ref[1] = (mix - high.astype(f32)).astype(bf16)


def add_kernel(own_ref, away_ref, out_ref, scratch, *, wire):
    groups = own_ref.shape[0]

    def get(message, column):
        block, group = divmod(message, groups)
        rows = slice(block * wire.pad, (block + 1) * wire.pad)
        lanes = wire.block(column)
        return own_ref[group, rows, lanes] + away_ref[group, rows, lanes].astype(jnp.float32)

    wire.pack(scratch, out_ref, get)


def combine_kernel(back_ref, mix_ref, out_ref, *, wire):
    tok_count = out_ref.shape[0]
    total = dot(mix_ref[0], back_ref[...]) + dot(mix_ref[1], back_ref[...])
    for column in range(wire.columns):
        rows = total[column * tok_count : (column + 1) * tok_count]
        out_ref[:, wire.block(column)] = rows.astype(jnp.bfloat16)


def in_hbm(array):
    return pltpu.with_memory_space_constraint(array, pltpu.HBM)


def call(kernel, out_shape, args, flops, moved, scratch=(), spaces=None, limit=16 * MIB):
    specs = spaces or [SMEM if a.dtype == jnp.int32 and a.ndim == 1 else VMEM for a in args]
    return pl.pallas_call(
        kernel,
        out_shape=out_shape,
        in_specs=specs,
        out_specs=jax.tree.map(lambda _: VMEM, out_shape),
        scratch_shapes=scratch,
        compiler_params=pltpu.CompilerParams(vmem_limit_bytes=limit),
        cost_estimate=pl.CostEstimate(flops=flops, bytes_accessed=moved, transcendentals=0),
    )(*args)


def local(tokens, norm_gain, routing, route_weight, w_gate, w_up, w_down):
    tok_count, width = tokens.shape
    top_count = routing.shape[1]
    blocks = lax.axis_size("ep")
    groups = lax.axis_size("y")
    experts = blocks * w_gate.shape[0]
    hidden_width = w_gate.shape[2]
    capacity = max(2, tok_count * top_count // experts + 1)
    half = width // CORES
    share = width // (groups * CORES)
    there = Wire(blocks, capacity, half)
    home = Wire(blocks * groups, capacity, share)
    rows = blocks * there.pad
    core = lax.axis_index("core").reshape(1)
    swap = [(i, CORES - 1 - i) for i in range(CORES)]
    routes = routing.T
    weights = route_weight.T
    bf16, f32 = jnp.bfloat16, jnp.float32
    shape = jax.ShapeDtypeStruct

    sending = call(
        functools.partial(gather_kernel, wire=there),
        shape((there.rows, there.lanes), bf16),
        (core, *[in_hbm(a) for a in (tokens, norm_gain.reshape(1, width), routes)]),
        40 * 10**9,
        60 * 10**6,
        scratch=(
            pltpu.VMEM((tok_count, width), bf16),
            pltpu.VMEM((1, width), f32),
            pltpu.VMEM((top_count, tok_count), jnp.int32),
            there.scratch(),
            pltpu.SemaphoreType.DMA((3,)),
        ),
        spaces=[SMEM, HBM, HBM, HBM],
    )
    own = lax.all_to_all(
        sending.reshape(blocks, there.stride, there.lanes),
        "ep",
        split_axis=0,
        concat_axis=0,
        tiled=True,
    ).reshape(there.rows, there.lanes)
    peer = lax.ppermute(own, "core", swap)
    pre = shape((rows, hidden_width), f32)
    step = 2 * rows * half * hidden_width
    unpacking = (there.scratch(), pltpu.VMEM((rows, half), bf16))
    gate_part, up_part = call(
        functools.partial(first_kernel, wire=there),
        (pre, pre),
        (core, own, w_gate, w_up, w_down),
        2 * step,
        4 * half * hidden_width,
        scratch=unpacking,
    )
    hidden, away = call(
        functools.partial(second_kernel, wire=there),
        (shape((rows, hidden_width), bf16), shape((groups, rows, share), bf16)),
        (core, peer, gate_part, up_part, w_gate, w_up, w_down),
        3 * step,
        6 * half * hidden_width,
        scratch=unpacking,
    )
    arrived = lax.ppermute(away, "core", swap)
    kept, mix = call(
        functools.partial(third_kernel, wire=home, experts=experts),
        (
            shape((groups, rows, share), f32),
            shape((2, home.columns * tok_count, home.rows), bf16),
        ),
        (core, hidden, w_down, routes, weights),
        step,
        2 * half * hidden_width,
    )
    summed = call(
        functools.partial(add_kernel, wire=home),
        shape((home.rows, home.lanes), bf16),
        (kept, arrived),
        rows * half,
        8 * rows * half,
        scratch=(home.scratch(),),
    )
    back = lax.all_to_all(
        summed.reshape(blocks * groups, home.stride, home.lanes),
        ("ep", "y"),
        split_axis=0,
        concat_axis=0,
        tiled=True,
    ).reshape(home.rows, home.lanes)
    return call(
        functools.partial(combine_kernel, wire=home),
        shape((tok_count, share), bf16),
        (back, mix),
        4 * rows * tok_count * half,
        4 * rows * half,
    )


def solution(mesh):
    blocks, shares = mesh.devices.shape
    split = Mesh(mesh.devices.reshape(blocks, shares // CORES, CORES), ("ep", "y", "core"))
    tp = ("y", "core")
    placed = (
        P("ep", None),
        P(),
        P("ep", None),
        P("ep", None),
        P("ep", None, tp),
        P("ep", None, tp),
        P("ep", tp, None),
    )
    return jax.shard_map(
        local, mesh=split, in_specs=placed, out_specs=P("ep", tp), check_vma=False
    )
```

time: 46 us -> 41.3 us (0.90)
  local copies, waits for them, and re-layouts: 2.89 us -> 0.02 us
  blocking collectives: 36.4 us -> 33.7 us
  Pallas kernels: 4.09 us -> 5.64 us
  waiting for transfers between devices: 2.1 us -> 1.44 us
    unnamed x18 -> x10, local copies, waits for them, and re-layouts: 2.89 us -> 0.02 us
    all_to_all x2, blocking collectives: 36.4 us -> 33.7 us  [the longest x1 18.3 us: local(): lax.all_to_all(sending.reshape(blocks, there.stride, there.lanes), 'ep',...]
    pallas_call x6, Pallas kernels: 4.09 us -> 5.64 us  [call(): pl.pallas_call(kernel, out_shape=out_shape, in_specs=specs, out_specs=jax...]
    ppermute x1, waiting for transfers between devices: 1.19 us -> 0.7 us  [local(): arrived = lax.ppermute(away, 'core', swap)]
  transfers between devices with their start and end apart: 2 -> 2, of which waited for: 2 -> 2; matrix products, arithmetic and copies ran while one was open for 0% -> 0% of each run, Pallas kernels for 3% -> 4%
where the time goes in v2:
time: 41.3 us; the launch traced here: 41.1 us
  blocking collectives  33.7 us (82%)
  Pallas kernels  5.64 us (14%)
  waiting for transfers between devices  1.44 us (3%)
    all_to_all x1, blocking collectives, local(): lax.all_to_all(sending.reshape(blocks, there.stride, there.lanes), 'ep',...  18.3 us
    all_to_all x1, blocking collectives, local(): lax.all_to_all(summed.reshape(blocks * groups, home.stride, home.lanes),...  15.5 us
    pallas_call x6, Pallas kernels, call(): pl.pallas_call(kernel, out_shape=out_shape, in_specs=specs, out_specs=jax...  5.64 us
  transfers between devices with their start and end apart: 2, of which 2 were waited for; matrix products, arithmetic and copies ran while one was open for 0% of the time, Pallas kernels for 4%

profile of v2, /device:TPU:0, one launch (start us, length us, event | category | flops | bytes accessed | tf_op | source)
XLA Modules:
  0.0 41.1 jit_solution(12571592391119206174)
XLA Ops:
  0.0 0.0 copy-start
  0.0 0.0 copy-start.1
  0.0 0.0 copy-start.2
  0.0 1.5 %shard_map.73 = bf16[1280,128]{1,0:T(8,128)(2,1)S(1)} custom-call(s32[1]{0:T(128)} %bitcast.core_ref, bf16[24,3072]{1,0:T(8,128)(2,1)} %tok_hbm.1, f32[1,3072]{1,0:T(1,128)} %bitcast.16, s32[4,24]{1,0:T(4,128)} %bitcast.13), custom_call_target="tpu_custom_call" | custom-call | flops 40000000000 | bytes 60000000 | tf_op jit(solution)/shard_map/pallas_call | solution.py:245
  1.5 18.3 %all_to_all.10 = bf16[8,160,128]{2,1,0:T(8,128)(2,1)S(1)} all-to-all(bf16[8,160,128]{2,1,0:T(8,128)(2,1)S(1)} %bitcast.12), channel_id=1, replica_groups=mesh['ep'=8,'y'=2,'core'=2] {'ep'}, dimensions={0} | all-to-all | bytes 655360 | tf_op jit(solution)/shard_map/all_to_all | solution.py:291
  19.8 0.0 collective-permute-start
  19.8 0.0 copy-done
  19.8 0.0 copy-done.1
  19.8 0.0 copy-done.2
  19.8 0.9 %shard_map.74 = (f32[128,768]{1,0:T(8,128)S(1)}, f32[128,768]{1,0:T(8,128)S(1)}) custom-call(s32[1]{0:T(128)} %bitcast.core_ref, bf16[1280,128]{1,0:T(8,128)(2,1)S(1)} %bitcast.11, bf16[1,3072,768]{2,1,0:T(8,128)(2,1)S(1)} %copy-done.1, bf16[1,3072,768]{2,1,0:T(8,128)(2,1)S(1)} %copy-done.2, bf16[1,768,3072]{2,1,0:T(8,128)(2,1)S(1)} %copy-done), custom_call_target="tpu_custom_call" | custom-call | flops 603979776 | bytes 4718592 | tf_op jit(solution)/shard_map/pallas_call | solution.py:245
  20.7 0.7 %collective-permute-done.wire_ref = bf16[1280,128]{1,0:T(8,128)(2,1)S(1)} collective-permute-done((bf16[1280,128]{1,0:T(8,128)(2,1)S(1)}, bf16[1280,128]{1,0:T(8,128)(2,1)S(1)}, u32[]{:S(2)}, u32[]{:S(2)}) %collective-permute-start) | collective-permute-done | bytes 327712 | tf_op jit(solution)/shard_map/ppermute | solution.py:298
  21.4 0.0 copy-start.3
  21.4 0.0 copy-start.4
  21.4 1.3 %shard_map.75 = (bf16[128,768]{1,0:T(8,128)(2,1)S(1)}, bf16[2,128,768]{2,1,0:T(8,128)(2,1)S(1)}) custom-call(s32[1]{0:T(128)} %bitcast.core_ref, bf16[1280,128]{1,0:T(8,128)(2,1)S(1)} %collective-permute-done.wire_ref, f32[128,768]{1,0:T(8,128)S(1)} %get-tuple-element.11.gate_in, f32[128,768]{1,0:T(8,128)S(1)} %get-tuple-element.12.up_in, ...), custom_call_target="tpu_custom_call" | custom-call | flops 905969664 | bytes 7077888 | tf_op jit(solution)/shard_map/pallas_call | solution.py:245
  22.8 0.2 collective-permute-start.1
  23.0 0.0 copy-done.3
  23.0 0.0 copy-done.4
  23.0 0.9 %shard_map.76 = (f32[2,128,768]{2,1,0:T(8,128)S(1)}, bf16[2,144,1280]{2,1,0:T(8,128)(2,1)S(1)}) custom-call(s32[1]{0:T(128)} %bitcast.core_ref, bf16[128,768]{1,0:T(8,128)(2,1)S(1)} %get-tuple-element.13.hidden_ref, bf16[1,768,3072]{2,1,0:T(8,128)(2,1)S(1)} %copy-done, s32[4,24]{1,0:T(4,128)S(1)} %bitcast.14, f32[4,24]{1,0:T(4,128)S(1)} %bitcast.15), custom_call_target="tpu_custom_call" | custom-call | flops 301989888 | bytes 2359296 | tf_op jit(solution)/shard_map/pallas_call | solution.py:245
  23.8 0.7 %collective-permute-done.1.away_ref = bf16[2,128,768]{2,1,0:T(8,128)(2,1)S(1)} collective-permute-done((bf16[2,128,768]{2,1,0:T(8,128)(2,1)S(1)}, bf16[2,128,768]{2,1,0:T(8,128)(2,1)S(1)}, u32[]{:S(2)}, u32[]{:S(2)}) %collective-permute-start.1) | collective-permute-done | bytes 393248 | tf_op jit(solution)/shard_map/ppermute | solution.py:318
  24.5 0.1 shard_map.77
  24.7 15.5 %all_to_all.11 = bf16[16,80,128]{2,1,0:T(8,128)(2,1)S(1)} all-to-all(bf16[16,80,128]{2,1,0:T(8,128)(2,1)S(1)} %bitcast.9), channel_id=1, replica_groups=mesh['ep'=8,'y'=2,'core'=2] {'ep','y'}, dimensions={0} | all-to-all | bytes 655360 | tf_op jit(solution)/shard_map/all_to_all | solution.py:337
  40.2 1.0 %shard_map.78 = bf16[24,768]{1,0:T(8,128)(2,1)} custom-call(bf16[1280,128]{1,0:T(8,128)(2,1)S(1)} %bitcast.8, bf16[2,144,1280]{2,1,0:T(8,128)(2,1)S(1)} %get-tuple-element.16.mix_ref), custom_call_target="tpu_custom_call" | custom-call | flops 18874368 | bytes 786432 | tf_op jit(solution)/shard_map/pallas_call | solution.py:245
Async XLA Ops:
  0.0 19.8 %copy-start = (bf16[1,768,3072]{2,1,0:T(8,128)(2,1)S(1)}, bf16[1,768,3072]{2,1,0:T(8,128)(2,1)}, u32[]{:S(2)}) copy-start(bf16[1,768,3072]{2,1,0:T(8,128)(2,1)} %down_ref.3) | copy-start | bytes 14155780
  0.0 19.8 %copy-start.1 = (bf16[1,3072,768]{2,1,0:T(8,128)(2,1)S(1)}, bf16[1,3072,768]{2,1,0:T(8,128)(2,1)}, u32[]{:S(2)}) copy-start(bf16[1,3072,768]{2,1,0:T(8,128)(2,1)} %gate_ref.3) | copy-start | bytes 14155780
  0.0 19.8 %copy-start.2 = (bf16[1,3072,768]{2,1,0:T(8,128)(2,1)S(1)}, bf16[1,3072,768]{2,1,0:T(8,128)(2,1)}, u32[]{:S(2)}) copy-start(bf16[1,3072,768]{2,1,0:T(8,128)(2,1)} %up_ref.3) | copy-start | bytes 14155780
  19.8 1.6 %collective-permute-start = (bf16[1280,128]{1,0:T(8,128)(2,1)S(1)}, bf16[1280,128]{1,0:T(8,128)(2,1)S(1)}, u32[]{:S(2)}, u32[]{:S(2)}) collective-permute-start(bf16[1280,128]{1,0:T(8,128)(2,1)S(1)} %bitcast.10), channel_id=1, source_target_pairs={{0,1},{1,0},{2,3},{3,2},{4,5},{5,4},{6,7},{7,6},{8,9},{9,8},{10,11... | collective-permute-start | bytes 983048 | tf_op jit(solution)/shard_map/ppermute | solution.py:298
  21.4 1.6 %copy-start.3 = (s32[24,4]{0,1:T(4,128)S(1)}, s32[24,4]{0,1:T(4,128)}, u32[]{:S(2)}) copy-start(s32[24,4]{0,1:T(4,128)} %param.9) | copy-start | bytes 1156
  21.4 1.6 %copy-start.4 = (f32[24,4]{0,1:T(4,128)S(1)}, f32[24,4]{0,1:T(4,128)}, u32[]{:S(2)}) copy-start(f32[24,4]{0,1:T(4,128)} %param.10) | copy-start | bytes 1156
  22.8 1.8 %collective-permute-start.1 = (bf16[2,128,768]{2,1,0:T(8,128)(2,1)S(1)}, bf16[2,128,768]{2,1,0:T(8,128)(2,1)S(1)}, u32[]{:S(2)}, u32[]{:S(2)}) collective-permute-start(bf16[2,128,768]{2,1,0:T(8,128)(2,1)S(1)} %get-tuple-element.15), channel_id=1, source_target_pairs={{0,1},{1,0},{2,3},{3,2},{4,5},{5,4},{6,7},{7,6},{8,9},{9,8},{10,11... | collective-permute-start | bytes 1179656 | tf_op jit(solution)/shard_map/ppermute | solution.py:318
